TPU v7x, 32 devices: a whole 2x2x4 slice. The times are simulated.
32 devices in a mesh: row: 8 (over z, core), col: 4 (over y, x).
Axes of the slice: x: 2, y: 2, z: 4, core: 2. Of those that a mesh axis runs over, the one named last changes fastest.
Arguments:
- mix_input: bfloat16 [4, 2048, 1024], P('col', 'row'), may hold values from -6 to 6
- gate_logits: bfloat16 [4, 2048, 2048], P('col', 'row'), may hold values from -8 to 8
- w_proj: bfloat16 [1024, 2048], P('col'), may hold values from -0.1875 to 0.1875
Outputs:
- mixed: bfloat16 [4, 2048, 2048], P('col', 'row')
All inputs are finite; a program needn't handle non-finite values.
Results may differ from a plain program's by a relative error of at most 0.0049.
Values may be sent and summed in bfloat16 or wider, within the bound.
A program may use at most 64 MiB of HBM per device.

v0:
```python
import math
import jax
import jax.numpy as jnp
from jax import lax
from jax.sharding import PartitionSpec as P

GROUP = 256
GROUPS = 4
POS_INNER = 128
highest = lax.Precision.HIGHEST


def tables(rows_in, cols_out, period):
    left_index = jnp.arange(rows_in, dtype=jnp.int32)[:, None]
    right_index = jnp.arange(cols_out, dtype=jnp.int32)[None, :]
    angles = (left_index * right_index % period).astype(jnp.float32) * (2.0 * math.pi / period)
    return (jnp.cos(angles), jnp.sin(angles))


def half_tables(group_size):
    index_row = jnp.arange(group_size, dtype=jnp.int32)
    frequency = jnp.where(index_row == 1, group_size // 2, index_row // 2)
    is_cosine = jnp.logical_or(index_row % 2 == 0, index_row == 1)
    channel = jnp.arange(group_size, dtype=jnp.int32)[:, None]
    angles = (channel * frequency[None, :] % group_size).astype(jnp.float32) * (
        2.0 * math.pi / group_size
    )
    return jnp.where(is_cosine[None, :], jnp.cos(angles), jnp.sin(angles))


def position_transform(values, inner_len):
    length, columns = values.shape
    outer_len = length // inner_len
    blocks = values.reshape(inner_len, outer_len, columns)
    cos_one, sin_one = tables(inner_len, inner_len, inner_len)
    first_re = jnp.einsum("pqc,pk->ckq", blocks, cos_one, precision=highest)
    first_im = -jnp.einsum("pqc,pk->ckq", blocks, sin_one, precision=highest)
    cos_twist, sin_twist = tables(inner_len, outer_len, length)
    second_re = first_re * cos_twist + first_im * sin_twist
    second_im = first_im * cos_twist - first_re * sin_twist
    cos_two, sin_two = tables(outer_len, outer_len, outer_len)
    whole_re = jnp.einsum("ckq,qj->cjk", second_re, cos_two, precision=highest) + jnp.einsum(
        "ckq,qj->cjk", second_im, sin_two, precision=highest
    )
    whole_im = jnp.einsum("ckq,qj->cjk", second_im, cos_two, precision=highest) - jnp.einsum(
        "ckq,qj->cjk", second_re, sin_two, precision=highest
    )
    return (whole_re.reshape(columns, length), whole_im.reshape(columns, length))


def on_device(mix_input, gate_logits, w_proj):
    tokens = mix_input[0]
    tok_count, features = tokens.shape
    row_count = lax.axis_size("row")
    length = tok_count * row_count
    norm_factor = 1.0 / math.sqrt(length * GROUP)
    grouped = tokens.astype(jnp.float32).reshape(tok_count, GROUPS, GROUP)
    packed = jnp.einsum("tgc,cm->tgm", grouped, half_tables(GROUP), precision=highest).reshape(
        tok_count, features
    )
    packed_cols = lax.all_to_all(packed, "row", split_axis=1, concat_axis=0, tiled=True)
    part_re, part_im = position_transform(packed_cols, POS_INNER)
    columns = part_re.shape[0]
    pair_re = part_re.reshape(columns // 2, 2, length)
    pair_im = part_im.reshape(columns // 2, 2, length)
    pair_index = lax.axis_index("row") * (columns // 2) + jnp.arange(columns // 2, dtype=jnp.int32)
    special = (pair_index % (GROUP // 2) == 0)[:, None]
    low_half = jnp.where(special, pair_re[:, 0], pair_re[:, 0] + pair_im[:, 1])
    high_half = jnp.where(special, pair_re[:, 1], pair_re[:, 0] - pair_im[:, 1])
    paired = (
        jnp.stack([low_half, high_half], axis=1).reshape(columns, length) * norm_factor
    ).astype(jnp.bfloat16)
    returned = lax.all_to_all(paired, "row", split_axis=1, concat_axis=0, tiled=True)
    pair_grid = returned.reshape(GROUPS, GROUP // 2, 2, tok_count)
    spectrum = jnp.concatenate(
        [pair_grid[:, :, 0], pair_grid[:, :1, 1], jnp.flip(pair_grid[:, 1:, 1], axis=1)], axis=1
    ).reshape(features, tok_count)
    projected = lax.dot_general(
        spectrum,
        lax.all_gather(w_proj, "col", axis=0, tiled=True),
        (((0,), (0,)), ((), ())),
        preferred_element_type=jnp.float32,
    )
    gate_open = jax.nn.sigmoid(gate_logits[0].astype(jnp.float32))
    return (gate_open * projected).astype(jnp.bfloat16)[None]


def solution(mesh):
    in_specs = (P("col", "row", None), P("col", "row", None), P("col", None))
    out_specs = P("col", "row", None)
    return jax.shard_map(
        on_device, mesh=mesh, in_specs=in_specs, out_specs=out_specs, check_vma=False
    )
```

profile of v0, /device:TPU:0, one launch (start us, length us, event | category | flops | bytes accessed | tf_op | source)
XLA Modules:
  0.0 91.6 jit_solution(6947621169780344983)
XLA Ops:
  6.5 0.0 all-gather.2.cloned.1.call-start
  6.5 0.7 all-gather.2.cloned.1.call-update
  7.3 1.4 %reshape.125 = bf16[256,4,256]{2,1,0:T(4,128)(2,1)S(1)} reshape(bf16[1,256,1024]{2,1,0:T(8,128)(2,1)} %param.3) | data formatting | bytes 1048576 | tf_op jit(solution)/shard_map/reshape | solution.py:57
  8.7 1.7 %fusion.8 = f32[256,256,4]{1,0,2:T(8,128)S(1)} fusion(bf16[256,4,256]{2,1,0:T(4,128)(2,1)S(1)} %reshape.125, s32[256]{0:T(256)S(1)} %fusion.67, pred[256]{0:T(512)(128)(4,1)S(1)} %compare_or_fusion), kind=kOutput, calls=%fused_computation.18 | convolution fusion | flops 806289408 | bytes 1574144 | tf_op jit(solution)/shard_map/tgc,cm->tgm/dot_general | solution.py:58
  10.4 1.3 %copy.30 = f32[256,8,128]{2,0,1:T(8,128)} copy(f32[256,8,128]{0,2,1:T(8,128)S(1)} %bitcast.61) | data formatting | bytes 2097152 | tf_op jit(solution)/shard_map/all_to_all | solution.py:61
  11.7 6.4 %all-to-all-start = ((f32[256,8,128]{2,0,1:T(8,128)}), f32[256,8,128]{2,0,1:T(8,128)S(1)}, u32[]{:S(2)}, u32[]{:S(2)}) async-start(f32[256,8,128]{2,0,1:T(8,128)} %copy.30), calls=%async_computation | async-start | bytes 2097152 | tf_op jit(solution)/shard_map/all_to_all | solution.py:61
  18.1 0.1 fusion.59
  18.2 26.5 %all-to-all-done = f32[256,8,128]{2,0,1:T(8,128)S(1)} async-done(((f32[256,8,128]{2,0,1:T(8,128)}), f32[256,8,128]{2,0,1:T(8,128)S(1)}, u32[]{:S(2)}, u32[]{:S(2)}) %all-to-all-start) | async-done | bytes 1048608 | tf_op jit(solution)/shard_map/all_to_all | solution.py:61
  44.6 1.5 %convolution_negate_fusion = f32[128,16,128]{2,0,1:T(8,128)S(1)} fusion(f32[128,16,128]{2,1,0:T(8,128)S(1)} %bitcast.56), kind=kOutput, calls=%fused_computation.7 | convolution fusion | flops 403144704 | bytes 2097152 | tf_op jit(solution)/shard_map/pqc,pk->ckq/dot_general | solution.py:37
  46.1 2.8 %subtract_bitcast_fusion = (f32[128,128,16]{0,1,2:T(8,128)S(1)}, f32[128,128,16]{0,1,2:T(8,128)}) fusion(f32[128,16,128]{2,0,1:T(8,128)S(1)} %convolution_negate_fusion, f32[128,16]{0,1:T(8,128)S(1)} %get-tuple-element.9, f32[128,16]{0,1:T(8,128)S(1)} %get-tuple-element.10, f32[128,16,128]{2,1,0:T(8,128)S(1)} %bitcast.57), kind=kOutput, calls=%fused_computation.10 | convolution fusion | flops 404455424 | bytes 4210688 | tf_op jit(solution)/shard_map/pqc,pk->ckq/dot_general | solution.py:36
  49.0 1.7 %copy.33 = f32[128,128,16]{1,2,0:T(8,128)S(1)} copy(f32[128,128,16]{0,1,2:T(8,128)} %get-tuple-element.6) | data formatting | bytes 2097152 | tf_op jit(solution)/shard_map/add | solution.py:39
  50.7 0.5 copy.34
  51.1 1.0 %fusion.51 = f32[16,128,128]{2,0,1:T(8,128)S(1)} fusion(f32[128,128,16]{1,2,0:T(8,128)S(1)} %copy.33), kind=kOutput, calls=%fused_computation.70 | convolution fusion | flops 50335232 | bytes 2097152 | tf_op jit(solution)/shard_map/ckq,qj->cjk/dot_general | solution.py:42
  52.2 1.1 %fusion.3 = f32[128,16,128]{2,1,0:T(8,128)S(1)} fusion(f32[16,128,128]{2,0,1:T(8,128)S(1)} %fusion.51, f32[128,128,16]{1,2,0:T(8,128)S(1)} %copy.34), kind=kOutput, calls=%fused_computation.6 | convolution fusion | flops 50597376 | bytes 3145728 | tf_op jit(solution)/shard_map/ckq,qj->cjk/dot_general | solution.py:42
  53.3 1.5 %reshape_reshape.6 = f32[64,2,2048]{2,1,0:T(2,128)} reshape(f32[128,16,128]{2,1,0:T(8,128)S(1)} %fusion.3) | data formatting | bytes 2097152 | tf_op jit(solution)/shard_map/reshape;reshape | solution.py:64
  54.8 1.0 %fusion.49 = f32[16,128,128]{2,0,1:T(8,128)S(1)} fusion(f32[128,128,16]{1,2,0:T(8,128)S(1)} %copy.34), kind=kOutput, calls=%fused_computation.68 | convolution fusion | flops 50335232 | bytes 2097152 | tf_op jit(solution)/shard_map/ckq,qj->cjk/dot_general | solution.py:45
  55.9 0.0 copy-start
  55.9 1.1 %fusion.2 = f32[128,16,128]{2,1,0:T(8,128)S(1)} fusion(f32[16,128,128]{2,0,1:T(8,128)S(1)} %fusion.49, f32[128,128,16]{1,2,0:T(8,128)S(1)} %copy.33), kind=kOutput, calls=%fused_computation.4 | convolution fusion | flops 50597376 | bytes 3145728 | tf_op jit(solution)/shard_map/ckq,qj->cjk/dot_general | solution.py:45
  57.0 0.5 reshape_reshape.7
  57.5 0.0 copy-done
  57.5 1.6 %broadcast_select_fusion.1 = (f32[64,1,2048]{2,1,0:T(1,128)S(1)}, f32[64,1,2048]{2,1,0:T(1,128)S(1)}) fusion(pred[64]{0:T(512)(128)(4,1)S(1)} %fusion.69, f32[64,2,2048]{2,1,0:T(2,128)S(1)} %reshape_reshape.7, f32[64,2,2048]{2,1,0:T(2,128)S(1)} %copy-done), kind=kLoop, calls=%fused_computation.13 | loop fusion | flops 524288 | bytes 2621504 | tf_op jit(solution)/shard_map/jit(_where)/select_n | solution.py:68
  59.1 1.1 %fusion.4 = bf16[64,2,2048]{2,1,0:T(2,128)(2,1)S(1)} fusion(f32[64,1,2048]{2,1,0:T(1,128)S(1)} %get-tuple-element.8, f32[64,1,2048]{2,1,0:T(1,128)S(1)} %get-tuple-element.7), kind=kLoop, calls=%fused_computation.9 | loop fusion | flops 786432 | bytes 1572864 | tf_op jit(solution)/shard_map/convert_element_type | solution.py:72
  60.2 0.3 convert_element_type.54
  60.6 0.1 copy.37
  60.7 18.0 %all_to_all.29 = bf16[128,8,256]{2,0,1:T(8,128)(2,1)S(1)} all-to-all(bf16[128,8,256]{2,0,1:T(8,128)(2,1)S(1)} %copy.37), channel_id=1, replica_groups=mesh['row'=8,'col'=4] {'row'}, dimensions={1} | all-to-all | bytes 1048576 | tf_op jit(solution)/shard_map/all_to_all | solution.py:73
  78.6 0.2 reshape.127
  78.8 0.0 copy-start.1
  78.8 0.6 slice.32
  79.5 0.5 rev.4
  80.0 0.1 pad_maximum_fusion
  80.1 0.0 all-gather.2.cloned.1.call-done
  80.1 0.0 copy-done.1
  80.1 4.6 %fusion.1 = bf16[1,256,2048]{2,1,0:T(8,128)(2,1)} fusion(bf16[1024,256]{1,0:T(8,128)(2,1)S(1)} %bitcast.63, bf16[1024,2048]{1,0:T(8,128)(2,1)} %all-gather.2.cloned.1.call-done, bf16[1,256,2048]{2,1,0:T(8,128)(2,1)S(1)} %copy-done.1), kind=kOutput, calls=%fused_computation.2 | convolution fusion | flops 1076887552 | bytes 6815744 | tf_op jit(solution)/shard_map/dot_general | solution.py:78
  (6 shorter events, 0.1 us)
Async XLA Ops:
  6.5 73.6 %all-gather.2.cloned.1.call-start = ((), (), s32[]{:S(2)}) async-start(), calls=%async_computation.2 | async-start | bytes 5242880 | tf_op jit(solution)/shard_map/all_gather | solution.py:80
  11.7 32.9 %all-to-all-start = ((f32[256,8,128]{2,0,1:T(8,128)}), f32[256,8,128]{2,0,1:T(8,128)S(1)}, u32[]{:S(2)}, u32[]{:S(2)}) async-start(f32[256,8,128]{2,0,1:T(8,128)} %copy.30), calls=%async_computation | async-start | bytes 2097152 | tf_op jit(solution)/shard_map/all_to_all | solution.py:61
  55.9 1.7 %copy-start = (f32[64,2,2048]{2,1,0:T(2,128)S(1)}, f32[64,2,2048]{2,1,0:T(2,128)}, u32[]{:S(2)}) copy-start(f32[64,2,2048]{2,1,0:T(2,128)} %reshape_reshape.6) | copy-start | bytes 3145732
  78.8 1.3 %copy-start.1 = (bf16[1,256,2048]{2,1,0:T(8,128)(2,1)S(1)}, bf16[1,256,2048]{2,1,0:T(8,128)(2,1)}, u32[]{:S(2)}) copy-start(bf16[1,256,2048]{2,1,0:T(8,128)(2,1)} %param.4) | copy-start | bytes 3145732
Sparse Core Ops, SparseCore 0:
  9.2 55.2 all-gather.1
where the time goes:
time: 91.9 us; the launch traced here: 91.6 us
  waiting for transfers between devices  27.2 us (30%)
  blocking collectives  18 us (20%)
  matrix products  14.9 us (16%)
  between operations  13.6 us (15%)
  local copies, waits for them, and re-layouts  8.74 us (10%)
  starting transfers between devices  6.36 us (7%)
  other arithmetic  2.85 us (3%)
    all_to_all x1, waiting for transfers between devices, on_device(): lax.all_to_all(packed, 'row', split_axis=1, concat_axis=0, tiled=True)  26.5 us
    all_to_all x1, blocking collectives, on_device(): lax.all_to_all(paired, 'row', split_axis=1, concat_axis=0, tiled=True)  18 us
    all_to_all x1, starting transfers between devices, on_device(): lax.all_to_all(packed, 'row', split_axis=1, concat_axis=0, tiled=True)  6.35 us
    dot_general x1, matrix products, on_device(): lax.dot_general(spectrum, lax.all_gather(w_proj, 'col', axis=0, tiled=Tru...  4.64 us
    dot_general x1, matrix products, position_transform(): first_re = jnp.einsum('pqc,pk->ckq', blocks, cos_one, precision=highest)  2.84 us
  transfers between devices with their start and end apart: 2, of which 1 were waited for; matrix products, arithmetic and copies ran while one was open for 24% of the time, Pallas kernels for 0%

commit v1 on v0

--- a/solution.py
+++ b/solution.py
@@ -8,6 +8,17 @@
 GROUPS = 4
 POS_INNER = 128
 highest = lax.Precision.HIGHEST
+
+
+def cut_along(x, dim, size):
+    before, after = (x.shape[:dim], x.shape[dim + 1 :])
+    return jnp.moveaxis(x.reshape(*before, size, -1, *after), dim, 0)
+
+
+def in_order(pieces, dim):
+    pieces = jnp.moveaxis(pieces, 0, dim)
+    dims = pieces.shape
+    return pieces.reshape(*dims[:dim], dims[dim] * dims[dim + 1], *dims[dim + 2 :])
 
 
 def tables(rows_in, cols_out, period):
@@ -58,7 +69,16 @@
     packed = jnp.einsum("tgc,cm->tgm", grouped, half_tables(GROUP), precision=highest).reshape(
         tok_count, features
     )
-    packed_cols = lax.all_to_all(packed, "row", split_axis=1, concat_axis=0, tiled=True)
+    length_2, place = (lax.axis_size("row"), lax.axis_index("row"))
+    pieces = cut_along(packed, 1, length_2)
+    gathered = [pieces[place]]
+    for step in range(1, length_2):
+        sent = pieces[(place + step) % length_2]
+        gathered.append(
+            lax.ppermute(sent, "row", [(i, (i + step) % length_2) for i in range(length_2)])
+        )
+    pieces = jnp.stack(gathered)[(place - jnp.arange(length_2)) % length_2]
+    packed_cols = in_order(pieces, 0)
     part_re, part_im = position_transform(packed_cols, POS_INNER)
     columns = part_re.shape[0]
     pair_re = part_re.reshape(columns // 2, 2, length)

time: 91.9 us -> 87.1 us (0.948)
  waiting for transfers between devices: 27.2 us -> 8.73 us
  blocking collectives: 18 us -> 25.8 us
  starting transfers between devices: 6.36 us -> 11.6 us
    all_to_all x1 -> x0, waiting for transfers between devices: 26.5 us -> none  [on_device(): lax.all_to_all(packed, 'row', split_axis=1, concat_axis=0, tiled=True)]
    ppermute x0 -> x7, starting transfers between devices: none -> 11.6 us  [on_device(): lax.ppermute(sent, 'row', [(i, (i + step) % length_2) for i in range(leng...]
    ppermute x0 -> x7, waiting for transfers between devices: none -> 8 us  [on_device(): lax.ppermute(sent, 'row', [(i, (i + step) % length_2) for i in range(leng...]
    all_to_all x1, blocking collectives: 18 us -> 25.8 us  [on_device(): lax.all_to_all(paired, 'row', split_axis=1, concat_axis=0, tiled=True)]
    all_to_all x1 -> x0, starting transfers between devices: 6.35 us -> none  [on_device(): lax.all_to_all(packed, 'row', split_axis=1, concat_axis=0, tiled=True)]
    all_to_all x1 -> x0, local copies, waits for them, and re-layouts: 1.31 us -> none  [on_device(): lax.all_to_all(packed, 'row', split_axis=1, concat_axis=0, tiled=True)]
  transfers between devices with their start and end apart: 2 -> 8, of which waited for: 1 -> 3; matrix products, arithmetic and copies ran while one was open for 24% -> 26% of each run, Pallas kernels for 0% -> 0%
where the time goes in v1:
time: 87.1 us; the launch traced here: 86.9 us
  blocking collectives  25.8 us (30%)
  matrix products  14.8 us (17%)
  between operations  13.9 us (16%)
  starting transfers between devices  11.6 us (13%)
  local copies, waits for them, and re-layouts  8.98 us (10%)
  waiting for transfers between devices  8.73 us (10%)
  other arithmetic  3.1 us (4%)
    all_to_all x1, blocking collectives, on_device(): lax.all_to_all(paired, 'row', split_axis=1, concat_axis=0, tiled=True)  25.8 us
    ppermute x7, starting transfers between devices, on_device(): lax.ppermute(sent, 'row', [(i, (i + step) % length_2) for i in range(leng...  11.6 us
    ppermute x7, waiting for transfers between devices, on_device(): lax.ppermute(sent, 'row', [(i, (i + step) % length_2) for i in range(leng...  8 us
    dot_general x1, matrix products, on_device(): lax.dot_general(spectrum, lax.all_gather(w_proj, 'col', axis=0, tiled=Tru...  4.64 us
    dot_general x1, matrix products, position_transform(): first_re = jnp.einsum('pqc,pk->ckq', blocks, cos_one, precision=highest)  2.79 us
    select_n x1, other arithmetic, on_device(): low_half = jnp.where(special, pair_re[:, 0], pair_re[:, 0] + pair_im[:, 1])  1.78 us
  transfers between devices with their start and end apart: 8, of which 3 were waited for; matrix products, arithmetic and copies ran while one was open for 26% of the time, Pallas kernels for 0%

profile of v1, /device:TPU:0, one launch (start us, length us, event | category | flops | bytes accessed | tf_op | source)
XLA Modules:
  0.0 86.9 jit_solution(7564460208654972078)
XLA Ops:
  6.5 0.0 all-gather.2.cloned.1.call-start
  6.5 0.7 all-gather.2.cloned.1.call-update
  7.3 1.4 %reshape.180 = bf16[256,4,256]{2,1,0:T(4,128)(2,1)S(1)} reshape(bf16[1,256,1024]{2,1,0:T(8,128)(2,1)} %param.3) | data formatting | bytes 1048576 | tf_op jit(solution)/shard_map/reshape | solution.py:68
  8.7 1.7 %fusion.8 = f32[256,256,4]{1,0,2:T(8,128)S(1)} fusion(bf16[256,4,256]{2,1,0:T(4,128)(2,1)S(1)} %reshape.180, s32[256]{0:T(256)S(1)} %fusion.74, pred[256]{0:T(512)(128)(4,1)S(1)} %compare_or_fusion), kind=kOutput, calls=%fused_computation.19 | convolution fusion | flops 806289408 | bytes 1574144 | tf_op jit(solution)/shard_map/tgc,cm->tgm/dot_general | solution.py:69
  10.5 0.1 constant_dynamic-slice_fusion
  10.6 0.1 copy.37
  10.7 0.5 collective-permute-start
  11.3 0.1 copy.38
  11.3 2.6 %collective-permute-start.1 = (f32[256,128]{1,0:T(8,128)S(1)}, f32[256,128]{1,0:T(8,128)S(1)}, u32[]{:S(2)}, u32[]{:S(2)}) collective-permute-start(f32[256,128]{1,0:T(8,128)S(1)} %bitcast.90), channel_id=1, source_target_pairs={{0,8},{4,12},{8,16},{12,20},{16,24},{20,28},{24,0},{28,4},{1,9},{5... | collective-permute-start | bytes 393224 | tf_op jit(solution)/shard_map/ppermute | solution.py:78
  14.0 0.1 copy.39
  14.1 2.6 %collective-permute-start.2 = (f32[256,128]{1,0:T(8,128)S(1)}, f32[256,128]{1,0:T(8,128)S(1)}, u32[]{:S(2)}, u32[]{:S(2)}) collective-permute-start(f32[256,128]{1,0:T(8,128)S(1)} %bitcast.89), channel_id=1, source_target_pairs={{0,12},{4,16},{8,20},{12,24},{16,28},{20,0},{24,4},{28,8},{1,13},{... | collective-permute-start | bytes 393224 | tf_op jit(solution)/shard_map/ppermute | solution.py:78
  16.7 0.1 copy.40
  16.8 1.3 %collective-permute-start.3 = (f32[256,128]{1,0:T(8,128)S(1)}, f32[256,128]{1,0:T(8,128)S(1)}, u32[]{:S(2)}, u32[]{:S(2)}) collective-permute-start(f32[256,128]{1,0:T(8,128)S(1)} %bitcast.88), channel_id=1, source_target_pairs={{0,16},{4,20},{8,24},{12,28},{16,0},{20,4},{24,8},{28,12},{1,17},{... | collective-permute-start | bytes 393224 | tf_op jit(solution)/shard_map/ppermute | solution.py:78
  18.1 0.1 copy.41
  18.2 1.2 %collective-permute-start.4 = (f32[256,128]{1,0:T(8,128)S(1)}, f32[256,128]{1,0:T(8,128)S(1)}, u32[]{:S(2)}, u32[]{:S(2)}) collective-permute-start(f32[256,128]{1,0:T(8,128)S(1)} %bitcast.87), channel_id=1, source_target_pairs={{0,20},{4,24},{8,28},{12,0},{16,4},{20,8},{24,12},{28,16},{1,21},{... | collective-permute-start | bytes 393224 | tf_op jit(solution)/shard_map/ppermute | solution.py:78
  19.4 0.1 copy.36
  19.5 0.1 copy.42
  19.6 0.1 copy.43
  19.7 0.1 fusion.59
  19.8 0.0 collective-permute-done
  19.8 1.4 %collective-permute-start.5 = (f32[256,128]{1,0:T(8,128)S(1)}, f32[256,128]{1,0:T(8,128)S(1)}, u32[]{:S(2)}, u32[]{:S(2)}) collective-permute-start(f32[256,128]{1,0:T(8,128)S(1)} %bitcast.92), channel_id=1, source_target_pairs={{0,24},{4,28},{8,0},{12,4},{16,8},{20,12},{24,16},{28,20},{1,25},{... | collective-permute-start | bytes 393224 | tf_op jit(solution)/shard_map/ppermute | solution.py:78
  21.2 0.0 collective-permute-done.1
  21.3 1.9 %collective-permute-start.6 = (f32[256,128]{1,0:T(8,128)S(1)}, f32[256,128]{1,0:T(8,128)S(1)}, u32[]{:S(2)}, u32[]{:S(2)}) collective-permute-start(f32[256,128]{1,0:T(8,128)S(1)} %bitcast.91), channel_id=1, source_target_pairs={{0,28},{4,0},{8,4},{12,8},{16,12},{20,16},{24,20},{28,24},{1,29},{... | collective-permute-start | bytes 393224 | tf_op jit(solution)/shard_map/ppermute | solution.py:78
  23.1 7.4 %collective-permute-done.2 = f32[256,128]{1,0:T(8,128)S(1)} collective-permute-done((f32[256,128]{1,0:T(8,128)S(1)}, f32[256,128]{1,0:T(8,128)S(1)}, u32[]{:S(2)}, u32[]{:S(2)}) %collective-permute-start.2) | collective-permute-done | bytes 131104 | tf_op jit(solution)/shard_map/ppermute | solution.py:78
  30.5 0.2 collective-permute-done.3
  30.7 0.0 collective-permute-done.4
  30.8 0.0 collective-permute-done.5
  30.8 0.4 collective-permute-done.6
  31.2 0.6 gather_fusion
  31.9 1.5 %convolution_negate_fusion = f32[128,16,128]{2,0,1:T(8,128)S(1)} fusion(f32[128,16,128]{2,1,0:T(8,128)S(1)} %bitcast.79), kind=kOutput, calls=%fused_computation.8 | convolution fusion | flops 403144704 | bytes 2097152 | tf_op jit(solution)/shard_map/pqc,pk->ckq/dot_general | solution.py:48
  33.3 2.8 %subtract_bitcast_fusion = (f32[128,128,16]{0,1,2:T(8,128)S(1)}, f32[128,128,16]{0,1,2:T(8,128)}) fusion(f32[128,16,128]{2,0,1:T(8,128)S(1)} %convolution_negate_fusion, f32[128,16]{0,1:T(8,128)S(1)} %get-tuple-element.17, f32[128,16]{0,1:T(8,128)S(1)} %get-tuple-element.18, f32[128,16,128]{2,1,0:T(8,128)S(1)} %bitcast.80), kind=kOutput, calls=%fused_computation.11 | convolution fusion | flops 404455424 | bytes 4210688 | tf_op jit(solution)/shard_map/pqc,pk->ckq/dot_general | solution.py:47
  36.1 1.7 %copy.46 = f32[128,128,16]{1,2,0:T(8,128)S(1)} copy(f32[128,128,16]{0,1,2:T(8,128)} %get-tuple-element.6) | data formatting | bytes 2097152 | tf_op jit(solution)/shard_map/add | solution.py:50
  37.8 0.5 copy.47
  38.4 1.0 %fusion.51 = f32[16,128,128]{2,0,1:T(8,128)S(1)} fusion(f32[128,128,16]{1,2,0:T(8,128)S(1)} %copy.46), kind=kOutput, calls=%fused_computation.79 | convolution fusion | flops 50335232 | bytes 2097152 | tf_op jit(solution)/shard_map/ckq,qj->cjk/dot_general | solution.py:53
  39.4 1.0 %fusion.3 = f32[128,16,128]{2,1,0:T(8,128)S(1)} fusion(f32[16,128,128]{2,0,1:T(8,128)S(1)} %fusion.51, f32[128,128,16]{1,2,0:T(8,128)S(1)} %copy.47), kind=kOutput, calls=%fused_computation.7 | convolution fusion | flops 50597376 | bytes 3145728 | tf_op jit(solution)/shard_map/ckq,qj->cjk/dot_general | solution.py:53
  40.5 1.5 %reshape_reshape.14 = f32[64,2,2048]{2,1,0:T(2,128)} reshape(f32[128,16,128]{2,1,0:T(8,128)S(1)} %fusion.3) | data formatting | bytes 2097152 | tf_op jit(solution)/shard_map/reshape;reshape | solution.py:84
  42.0 1.0 %fusion.49 = f32[16,128,128]{2,0,1:T(8,128)S(1)} fusion(f32[128,128,16]{1,2,0:T(8,128)S(1)} %copy.47), kind=kOutput, calls=%fused_computation.77 | convolution fusion | flops 50335232 | bytes 2097152 | tf_op jit(solution)/shard_map/ckq,qj->cjk/dot_general | solution.py:56
  43.0 0.0 copy-start
  43.0 1.0 %fusion.2 = f32[128,16,128]{2,1,0:T(8,128)S(1)} fusion(f32[16,128,128]{2,0,1:T(8,128)S(1)} %fusion.49, f32[128,128,16]{1,2,0:T(8,128)S(1)} %copy.46), kind=kOutput, calls=%fused_computation.5 | convolution fusion | flops 50597376 | bytes 3145728 | tf_op jit(solution)/shard_map/ckq,qj->cjk/dot_general | solution.py:56
  44.1 0.5 reshape_reshape.15
  44.6 0.0 copy-done
  44.6 1.8 %broadcast_select_fusion.1 = (f32[64,1,2048]{2,1,0:T(1,128)S(1)}, f32[64,1,2048]{2,1,0:T(1,128)S(1)}) fusion(pred[64]{0:T(512)(128)(4,1)S(1)} %fusion.76, f32[64,2,2048]{2,1,0:T(2,128)S(1)} %reshape_reshape.15, f32[64,2,2048]{2,1,0:T(2,128)S(1)} %copy-done), kind=kLoop, calls=%fused_computation.14 | loop fusion | flops 524288 | bytes 2621504 | tf_op jit(solution)/shard_map/jit(_where)/select_n | solution.py:88
  46.4 1.1 %fusion.4 = bf16[64,2,2048]{2,1,0:T(2,128)(2,1)S(1)} fusion(f32[64,1,2048]{2,1,0:T(1,128)S(1)} %get-tuple-element.8, f32[64,1,2048]{2,1,0:T(1,128)S(1)} %get-tuple-element.7), kind=kLoop, calls=%fused_computation.10 | loop fusion | flops 786432 | bytes 1572864 | tf_op jit(solution)/shard_map/convert_element_type | solution.py:92
  47.6 0.3 convert_element_type.54
  47.9 0.1 copy.50
  48.0 25.8 %all_to_all.13 = bf16[128,8,256]{2,0,1:T(8,128)(2,1)S(1)} all-to-all(bf16[128,8,256]{2,0,1:T(8,128)(2,1)S(1)} %copy.50), channel_id=1, replica_groups=mesh['row'=8,'col'=4] {'row'}, dimensions={1} | all-to-all | bytes 1048576 | tf_op jit(solution)/shard_map/all_to_all | solution.py:93
  73.9 0.2 reshape.181
  74.1 0.0 copy-start.1
  74.1 0.6 slice.34
  74.7 0.5 rev.4
  75.2 0.1 pad_maximum_fusion
  75.3 0.0 all-gather.2.cloned.1.call-done
  75.4 0.0 copy-done.1
  75.4 4.6 %fusion.1 = bf16[1,256,2048]{2,1,0:T(8,128)(2,1)} fusion(bf16[1024,256]{1,0:T(8,128)(2,1)S(1)} %bitcast.86, bf16[1024,2048]{1,0:T(8,128)(2,1)} %all-gather.2.cloned.1.call-done, bf16[1,256,2048]{2,1,0:T(8,128)(2,1)S(1)} %copy-done.1), kind=kOutput, calls=%fused_computation.3 | convolution fusion | flops 1076887552 | bytes 6815744 | tf_op jit(solution)/shard_map/dot_general | solution.py:98
  (16 shorter events, 0.2 us)
Async XLA Ops:
  6.5 68.8 %all-gather.2.cloned.1.call-start = ((), (), s32[]{:S(2)}) async-start(), calls=%async_computation.1 | async-start | bytes 5242880 | tf_op jit(solution)/shard_map/all_gather | solution.py:100
  10.7 9.1 %collective-permute-start = (f32[256,128]{1,0:T(8,128)S(1)}, f32[256,128]{1,0:T(8,128)S(1)}, u32[]{:S(2)}, u32[]{:S(2)}) collective-permute-start(f32[256,128]{1,0:T(8,128)S(1)} %bitcast.93), channel_id=1, source_target_pairs={{0,4},{4,8},{8,12},{12,16},{16,20},{20,24},{24,28},{28,0},{1,5},{5... | collective-permute-start | bytes 393224 | tf_op jit(solution)/shard_map/ppermute | solution.py:78
  11.3 9.9 %collective-permute-start.1 = (f32[256,128]{1,0:T(8,128)S(1)}, f32[256,128]{1,0:T(8,128)S(1)}, u32[]{:S(2)}, u32[]{:S(2)}) collective-permute-start(f32[256,128]{1,0:T(8,128)S(1)} %bitcast.90), channel_id=1, source_target_pairs={{0,8},{4,12},{8,16},{12,20},{16,24},{20,28},{24,0},{28,4},{1,9},{5... | collective-permute-start | bytes 393224 | tf_op jit(solution)/shard_map/ppermute | solution.py:78
  14.1 16.4 %collective-permute-start.2 = (f32[256,128]{1,0:T(8,128)S(1)}, f32[256,128]{1,0:T(8,128)S(1)}, u32[]{:S(2)}, u32[]{:S(2)}) collective-permute-start(f32[256,128]{1,0:T(8,128)S(1)} %bitcast.89), channel_id=1, source_target_pairs={{0,12},{4,16},{8,20},{12,24},{16,28},{20,0},{24,4},{28,8},{1,13},{... | collective-permute-start | bytes 393224 | tf_op jit(solution)/shard_map/ppermute | solution.py:78
  16.8 13.9 %collective-permute-start.3 = (f32[256,128]{1,0:T(8,128)S(1)}, f32[256,128]{1,0:T(8,128)S(1)}, u32[]{:S(2)}, u32[]{:S(2)}) collective-permute-start(f32[256,128]{1,0:T(8,128)S(1)} %bitcast.88), channel_id=1, source_target_pairs={{0,16},{4,20},{8,24},{12,28},{16,0},{20,4},{24,8},{28,12},{1,17},{... | collective-permute-start | bytes 393224 | tf_op jit(solution)/shard_map/ppermute | solution.py:78
  18.2 12.5 %collective-permute-start.4 = (f32[256,128]{1,0:T(8,128)S(1)}, f32[256,128]{1,0:T(8,128)S(1)}, u32[]{:S(2)}, u32[]{:S(2)}) collective-permute-start(f32[256,128]{1,0:T(8,128)S(1)} %bitcast.87), channel_id=1, source_target_pairs={{0,20},{4,24},{8,28},{12,0},{16,4},{20,8},{24,12},{28,16},{1,21},{... | collective-permute-start | bytes 393224 | tf_op jit(solution)/shard_map/ppermute | solution.py:78
  19.8 10.9 %collective-permute-start.5 = (f32[256,128]{1,0:T(8,128)S(1)}, f32[256,128]{1,0:T(8,128)S(1)}, u32[]{:S(2)}, u32[]{:S(2)}) collective-permute-start(f32[256,128]{1,0:T(8,128)S(1)} %bitcast.92), channel_id=1, source_target_pairs={{0,24},{4,28},{8,0},{12,4},{16,8},{20,12},{24,16},{28,20},{1,25},{... | collective-permute-start | bytes 393224 | tf_op jit(solution)/shard_map/ppermute | solution.py:78
  21.3 10.0 %collective-permute-start.6 = (f32[256,128]{1,0:T(8,128)S(1)}, f32[256,128]{1,0:T(8,128)S(1)}, u32[]{:S(2)}, u32[]{:S(2)}) collective-permute-start(f32[256,128]{1,0:T(8,128)S(1)} %bitcast.91), channel_id=1, source_target_pairs={{0,28},{4,0},{8,4},{12,8},{16,12},{20,16},{24,20},{28,24},{1,29},{... | collective-permute-start | bytes 393224 | tf_op jit(solution)/shard_map/ppermute | solution.py:78
  43.0 1.6 %copy-start = (f32[64,2,2048]{2,1,0:T(2,128)S(1)}, f32[64,2,2048]{2,1,0:T(2,128)}, u32[]{:S(2)}) copy-start(f32[64,2,2048]{2,1,0:T(2,128)} %reshape_reshape.14) | copy-start | bytes 3145732
  74.1 1.3 %copy-start.1 = (bf16[1,256,2048]{2,1,0:T(8,128)(2,1)S(1)}, bf16[1,256,2048]{2,1,0:T(8,128)(2,1)}, u32[]{:S(2)}) copy-start(bf16[1,256,2048]{2,1,0:T(8,128)(2,1)} %param.4) | copy-start | bytes 3145732
Sparse Core Ops, SparseCore 0:
  9.2 55.2 all-gather.1
